TPU v7x, 512 devices: a whole 4x4x16 slice. The times are simulated.
512 devices in a mesh: fs: 32 (over z, core), tp: 16 (over y, x).
Axes of the slice: x: 4, y: 4, z: 16, core: 2. Of those that a mesh axis runs over, the one named last changes fastest.
Arguments:
- late_input: bfloat16 [4096, 2048], P('fs'), may hold values from -6 to 6
- early_input: bfloat16 [4096, 2048], P('fs'), may hold values from -6 to 6
- early_mid: bfloat16 [4096, 2048], P('fs'), may hold values from -6 to 6
- cotangent: bfloat16 [4096, 2048], P('fs'), may hold values from -6 to 6
- gain_first: float32 [2048], replicated, may hold values from 0.1 to 1.9
- gain_second: float32 [2048], replicated, may hold values from 0.1 to 1.9
- gate_first: bfloat16 [2048, 2816], P('fs', 'tp'), may hold values from -0.125 to 0.125
- up_first: bfloat16 [2048, 2816], P('fs', 'tp'), may hold values from -0.125 to 0.125
- down_first: bfloat16 [2816, 2048], P('tp', 'fs'), may hold values from -0.109375 to 0.109375
- gate_second: bfloat16 [2048, 2816], P('fs', 'tp'), may hold values from -0.125 to 0.125
- up_second: bfloat16 [2048, 2816], P('fs', 'tp'), may hold values from -0.125 to 0.125
- down_second: bfloat16 [2816, 2048], P('tp', 'fs'), may hold values from -0.109375 to 0.109375
- sum_gate_first: float32 [2048, 2816], P('fs', 'tp'), may hold values from -256 to 256
- sum_up_first: float32 [2048, 2816], P('fs', 'tp'), may hold values from -256 to 256
- sum_down_first: float32 [2816, 2048], P('tp', 'fs'), may hold values from -256 to 256
- sum_gate_second: float32 [2048, 2816], P('fs', 'tp'), may hold values from -256 to 256
- sum_up_second: float32 [2048, 2816], P('fs', 'tp'), may hold values from -256 to 256
- sum_down_second: float32 [2816, 2048], P('tp', 'fs'), may hold values from -256 to 256
Outputs:
- late_mid: bfloat16 [4096, 2048], P('fs')
- late_out: bfloat16 [4096, 2048], P('fs')
- input_grad: bfloat16 [4096, 2048], P('fs')
- new_gate_first: float32 [2048, 2816], P('fs', 'tp')
- new_up_first: float32 [2048, 2816], P('fs', 'tp')
- new_down_first: float32 [2816, 2048], P('tp', 'fs')
- new_gate_second: float32 [2048, 2816], P('fs', 'tp')
- new_up_second: float32 [2048, 2816], P('fs', 'tp')
- new_down_second: float32 [2816, 2048], P('tp', 'fs')
All inputs are finite; a program needn't handle non-finite values.
Results may differ from a plain program's by a relative error of at most 0.015.
Values may be sent and summed in bfloat16 or wider, within the bound.
No kernel may reach another device: no remote copies, remote signals or barrier semaphores. Data moves between devices by JAX's collectives and lax.ppermute only.
A program may use at most 128 MiB of HBM per device.

v0:
```python
import jax
import jax.numpy as jnp
from jax import lax
from jax.sharding import PartitionSpec as P

norm_eps = 1e-06


def sent_together(arrays, axis, dim, along):
    both = jnp.concatenate(arrays, axis=along)
    whole, at, outs = (lax.all_gather(both, axis, axis=dim, tiled=True), 0, [])
    for a in arrays:
        outs.append(lax.slice_in_dim(whole, at, at + a.shape[along], axis=along))
        at += a.shape[along]
    return tuple(outs)


def gather_turned(arrays, axis, dims):
    turned = [jnp.moveaxis(a, dim, 0) for a, dim in zip(arrays, dims)]
    widths = [t[0].size for t in turned]
    both = jnp.concatenate([t.reshape(-1, w) for t, w in zip(turned, widths)], axis=1)
    whole = lax.all_gather(both, axis, axis=0, tiled=True)
    blocks = jnp.split(whole, [sum(widths[:k]) for k in range(1, len(widths))], axis=1)
    return tuple(
        (
            jnp.moveaxis(b.reshape(-1, *t.shape[1:]), 0, dim)
            for b, t, dim in zip(blocks, turned, dims)
        )
    )


def normalize(values, gain_vector):
    widened = values.astype(jnp.float32)
    factor = lax.rsqrt(jnp.mean(widened * widened, axis=-1, keepdims=True) + norm_eps)
    normed = (widened * factor * gain_vector).astype(jnp.bfloat16)
    return (widened, factor, normed)


def block_forward(values, params):
    gain_vector, w_gate, w_up, w_down = params
    widened, factor, normed = normalize(values, gain_vector)
    gate_pre = jnp.dot(normed, w_gate, preferred_element_type=jnp.float32)
    up_pre = jnp.dot(normed, w_up, preferred_element_type=jnp.float32)
    hidden = (jax.nn.silu(gate_pre) * up_pre).astype(jnp.bfloat16)
    branch = lax.psum(
        jnp.dot(hidden, w_down, preferred_element_type=jnp.float32).astype(jnp.bfloat16), "tp"
    ).astype(jnp.float32)
    return (widened + 0.5 * branch).astype(jnp.bfloat16)


def block_backward(values, cotangent, params):
    gain_vector, w_gate, w_up, w_down = params
    widened, factor, normed = normalize(values, gain_vector)
    gate_pre = jnp.dot(normed, w_gate, preferred_element_type=jnp.float32)
    up_pre = jnp.dot(normed, w_up, preferred_element_type=jnp.float32)
    sigmoid_gate = jax.nn.sigmoid(gate_pre)
    activated = gate_pre * sigmoid_gate
    hidden = (activated * up_pre).astype(jnp.bfloat16)
    hidden_grad = 0.5 * jnp.einsum(
        "td,fd->tf", cotangent, w_down, preferred_element_type=jnp.float32
    )
    gate_grad = (
        hidden_grad * up_pre * sigmoid_gate * (1.0 + gate_pre * (1.0 - sigmoid_gate))
    ).astype(jnp.bfloat16)
    up_grad = (hidden_grad * activated).astype(jnp.bfloat16)
    partial_value = jnp.einsum("tf,df->td", gate_grad, w_gate, preferred_element_type=jnp.float32)
    partial_value = partial_value + jnp.einsum(
        "tf,df->td", up_grad, w_up, preferred_element_type=jnp.float32
    )
    normed_grad = lax.psum(partial_value.astype(jnp.bfloat16), "tp").astype(jnp.float32)
    scaled = normed_grad * gain_vector
    unit_rows = widened * factor
    rows_grad = cotangent.astype(jnp.float32) + factor * (
        scaled - unit_rows * jnp.mean(scaled * unit_rows, axis=-1, keepdims=True)
    )
    return (rows_grad, (normed, cotangent, gate_grad, up_grad, hidden))


def fold_pair(pieces, columns_in):
    return (
        jnp.einsum("td,tf->df", columns_in, pieces[0], preferred_element_type=jnp.float32),
        jnp.einsum("td,tf->df", columns_in, pieces[1], preferred_element_type=jnp.float32),
    )


def fold_block(pieces, columns_in, columns_out):
    paired = fold_pair(pieces[0:2], columns_in)
    return paired + (
        jnp.einsum("tf,td->fd", pieces[2], columns_out, preferred_element_type=jnp.float32),
    )


def per_device(
    late_input,
    early_input,
    early_mid,
    cotangent,
    gain_first,
    gain_second,
    gate_first,
    up_first,
    down_first,
    gate_second,
    up_second,
    down_second,
    sum_gate_first,
    sum_up_first,
    sum_down_first,
    sum_gate_second,
    sum_up_second,
    sum_down_second,
):
    rows_in = sent_together((gate_first, up_first, gate_second, up_second), "fs", 0, 1)
    cols_out = gather_turned((down_first, down_second), "fs", (1, 1))
    first_params = (gain_first, rows_in[0], rows_in[1], cols_out[0])
    second_params = (gain_second, rows_in[2], rows_in[3], cols_out[1])
    late_mid = block_forward(late_input, first_params)
    late_out = block_forward(late_mid, second_params)
    mid_grad, saved_second = block_backward(early_mid, cotangent, second_params)
    mid_grad = mid_grad.astype(jnp.bfloat16)
    rows_grad, saved_first = block_backward(early_input, mid_grad, first_params)
    pieces = sent_together(
        (
            saved_second[2],
            saved_second[3],
            saved_second[4],
            saved_first[2],
            saved_first[3],
            saved_first[4],
        ),
        "fs",
        0,
        1,
    )
    upper = fold_block(
        pieces[0:3],
        lax.all_to_all(saved_second[0], "fs", split_axis=1, concat_axis=0, tiled=True),
        lax.all_to_all(saved_second[1], "fs", split_axis=1, concat_axis=0, tiled=True),
    )
    lower = fold_block(
        pieces[3:6],
        lax.all_to_all(saved_first[0], "fs", split_axis=1, concat_axis=0, tiled=True),
        lax.all_to_all(saved_first[1], "fs", split_axis=1, concat_axis=0, tiled=True),
    )
    result = upper + lower
    grads_second = (result[0], result[1], 0.5 * result[2])
    grads_first = (result[3], result[4], 0.5 * result[5])
    return (
        late_mid,
        late_out,
        rows_grad.astype(jnp.bfloat16),
        sum_gate_first + grads_first[0],
        sum_up_first + grads_first[1],
        sum_down_first + grads_first[2],
        sum_gate_second + grads_second[0],
        sum_up_second + grads_second[1],
        sum_down_second + grads_second[2],
    )


def solution(mesh):
    in_specs = (
        P("fs", None),
        P("fs", None),
        P("fs", None),
        P("fs", None),
        P(),
        P(),
        P("fs", "tp"),
        P("fs", "tp"),
        P("tp", "fs"),
        P("fs", "tp"),
        P("fs", "tp"),
        P("tp", "fs"),
        P("fs", "tp"),
        P("fs", "tp"),
        P("tp", "fs"),
        P("fs", "tp"),
        P("fs", "tp"),
        P("tp", "fs"),
    )
    out_specs = (
        P("fs", None),
        P("fs", None),
        P("fs", None),
        P("fs", "tp"),
        P("fs", "tp"),
        P("tp", "fs"),
        P("fs", "tp"),
        P("fs", "tp"),
        P("tp", "fs"),
    )
    return jax.shard_map(
        per_device, mesh=mesh, in_specs=in_specs, out_specs=out_specs, check_vma=False
    )
```

profile of v0, /device:TPU:1, one launch (start us, length us, event | category | flops | bytes accessed | tf_op | source)
XLA Modules:
  0.0 560.9 jit_solution(5887314163387625684)
XLA Ops:
  16.1 71.3 %all-gather.6.cloned.1.call-done = bf16[2048,352]{1,0:T(8,128)(2,1)} async-done(((bf16[64,352]{1,0:T(8,128)(2,1)}), bf16[2048,352]{1,0:T(8,128)(2,1)}) %all-gather.6.cloned.1.call-update) | async-done | bytes 1441808 | tf_op jit(solution)/shard_map/all_gather | solution.py:22
  87.5 2.1 fusion.20
  89.6 70.4 %all-gather.4.cloned.1.call-done = bf16[2048,704]{1,0:T(8,128)(2,1)} async-done(((bf16[64,704]{1,0:T(8,128)(2,1)}), bf16[2048,704]{1,0:T(8,128)(2,1)}) %all-gather.4.cloned.1.call-update) | async-done | bytes 2883600 | tf_op jit(solution)/shard_map/all_gather | solution.py:11
  160.0 2.6 fusion.74
  162.6 3.2 constant_dynamic-update-slice_fusion.3
  168.1 3.9 convolution_convert_fusion.1
  177.5 110.1 %all-reduce.7.cloned.1.call-done = (bf16[128,2048]{1,0:T(8,128)(2,1)}, bf16[128,2048]{1,0:T(8,128)(2,1)}) async-done(((bf16[128,2048]{1,0:T(8,128)(2,1)}, bf16[128,2048]{1,0:T(8,128)(2,1)}), (bf16[128,2048]{1,0:T(8,128)(2,1)}, bf16[128,2048]{1,0:T(8,128)(2,1)})) %all-reduce.7.cloned.1.call-update) | async-done | bytes 1048592 | tf_op jit(solution)/shard_map/psum | solution.py:45
  297.6 4.0 convolution_convert_fusion
  306.4 14.7 %all-to-all-start = ((bf16[128,32,64]{0,2,1:T(8,128)(2,1)}), bf16[128,32,64]{0,2,1:T(8,128)(2,1)S(1)}, u32[]{:S(2)}, u32[]{:S(2)}) async-start(bf16[128,32,64]{0,2,1:T(8,128)(2,1)} %bitcast.3), calls=%async_computation | async-start | bytes 1048576 | tf_op jit(solution)/shard_map/all_to_all | solution.py:142
  322.2 32.5 %all-to-all-done = bf16[128,32,64]{0,2,1:T(8,128)(2,1)S(1)} async-done(((bf16[128,32,64]{0,2,1:T(8,128)(2,1)}), bf16[128,32,64]{0,2,1:T(8,128)(2,1)S(1)}, u32[]{:S(2)}, u32[]{:S(2)}) %all-to-all-start) | async-done | bytes 524320 | tf_op jit(solution)/shard_map/all_to_all | solution.py:142
  354.6 4.2 all-to-all-start.2
  359.8 32.5 %all-to-all-done.2 = bf16[128,32,64]{0,2,1:T(8,128)(2,1)S(1)} async-done(((bf16[128,32,64]{0,2,1:T(8,128)(2,1)}), bf16[128,32,64]{0,2,1:T(8,128)(2,1)S(1)}, u32[]{:S(2)}, u32[]{:S(2)}) %all-to-all-start.2) | async-done | bytes 524320 | tf_op jit(solution)/shard_map/all_to_all | solution.py:137
  392.3 5.0 all-to-all-start.1
  398.4 22.9 %all-reduce.5.cloned.1.call-done = (bf16[128,2048]{1,0:T(8,128)(2,1)}, bf16[128,2048]{1,0:T(8,128)(2,1)}) async-done(((bf16[128,2048]{1,0:T(8,128)(2,1)}, bf16[128,2048]{1,0:T(8,128)(2,1)}), (bf16[128,2048]{1,0:T(8,128)(2,1)}, bf16[128,2048]{1,0:T(8,128)(2,1)})) %all-reduce.5.cloned.1.call-update) | async-done | bytes 1048592 | tf_op jit(solution)/shard_map/psum | solution.py:45
  422.6 8.3 %all-to-all-done.1 = bf16[128,32,64]{0,2,1:T(8,128)(2,1)} async-done(((bf16[128,32,64]{0,2,1:T(8,128)(2,1)}), bf16[128,32,64]{0,2,1:T(8,128)(2,1)}, u32[]{:S(2)}, u32[]{:S(2)}) %all-to-all-start.1) | async-done | bytes 524320 | tf_op jit(solution)/shard_map/all_to_all | solution.py:143
  430.9 6.1 %all-to-all-start.3 = ((bf16[128,32,64]{0,2,1:T(8,128)(2,1)}), bf16[128,32,64]{0,2,1:T(8,128)(2,1)S(1)}, u32[]{:S(2)}, u32[]{:S(2)}) async-start(bf16[128,32,64]{0,2,1:T(8,128)(2,1)} %bitcast.9), calls=%async_computation.3 | async-start | bytes 1048576 | tf_op jit(solution)/shard_map/all_to_all | solution.py:138
  437.1 2.7 fusion.59
  439.8 98.8 %all-gather.8.cloned.1.call-done = bf16[4096,1056]{0,1:T(8,128)(2,1)} async-done(((bf16[128,1056]{0,1:T(8,128)(2,1)}), bf16[4096,1056]{0,1:T(8,128)(2,1)}) %all-gather.8.cloned.1.call-update) | async-done | bytes 8650768 | tf_op jit(solution)/shard_map/all_gather | solution.py:11
  538.7 2.6 fusion.23
  541.2 2.6 fusion.26
  543.9 2.6 fusion.35
  546.4 2.6 fusion.38
  549.1 2.7 fusion.32
  551.8 2.6 fusion.44
  (83 shorter events, 35.8 us)
Async XLA Ops:
  7.2 80.3 %all-gather.6.cloned.1.call-start = ((), (), s32[]{:S(2)}) async-start(), calls=%async_computation.5 | async-start | bytes 1622016 | tf_op jit(solution)/shard_map/all_gather | solution.py:22
  8.7 151.3 %all-gather.4.cloned.1.call-start = ((), (), s32[]{:S(2)}) async-start(), calls=%async_computation.4 | async-start | bytes 3244032 | tf_op jit(solution)/shard_map/all_gather | solution.py:11
  10.4 277.2 %all-reduce.7.cloned.1.call-start = ((), (), s32[]{:S(2)}) async-start(), calls=%async_computation.8 | async-start | bytes 2097152 | tf_op jit(solution)/shard_map/psum | solution.py:45
  16.1 150.4 %copy-start.12 = (f32[2048]{0:T(1024)S(1)}, f32[2048]{0:T(1024)}, u32[]{:S(2)}) copy-start(f32[2048]{0:T(1024)} %param.22) | copy-start | bytes 24580
  160.0 6.5 %copy-start = (bf16[2048,704]{1,0:T(8,128)(2,1)S(1)}, bf16[2048,704]{1,0:T(8,128)(2,1)}, u32[]{:S(2)}) copy-start(bf16[2048,704]{1,0:T(8,128)(2,1)} %all-gather.4.cloned.1.call-done) | copy-start | bytes 8650756
  174.1 115.2 %copy-start.11 = (f32[2048]{0:T(1024)S(1)}, f32[2048]{0:T(1024)}, u32[]{:S(2)}) copy-start(f32[2048]{0:T(1024)} %param.23) | copy-start | bytes 24580
  174.1 247.1 %all-reduce.5.cloned.1.call-start = ((), (), s32[]{:S(2)}) async-start(), calls=%async_computation.7 | async-start | bytes 2097152 | tf_op jit(solution)/shard_map/psum | solution.py:45
  287.6 6.5 %copy-start.6 = (bf16[128,2048]{1,0:T(8,128)(2,1)S(1)}, bf16[128,2048]{1,0:T(8,128)(2,1)}, u32[]{:S(2)}) copy-start(bf16[128,2048]{1,0:T(8,128)(2,1)} %copy-done.5) | copy-start | bytes 1572868
  289.2 6.6 %copy-start.8 = (bf16[128,2048]{1,0:T(8,128)(2,1)}, bf16[128,2048]{1,0:T(8,128)(2,1)S(1)}, u32[]{:S(2)}) copy-start(bf16[128,2048]{1,0:T(8,128)(2,1)S(1)} %get-tuple-element.22) | copy-start | bytes 1572868
  303.5 17.6 %copy-start.4 = (bf16[128,2048]{1,0:T(8,128)(2,1)S(1)}, bf16[128,2048]{1,0:T(8,128)(2,1)}, u32[]{:S(2)}) copy-start(bf16[128,2048]{1,0:T(8,128)(2,1)} %fusion.47) | copy-start | bytes 1572868
  303.5 55.3 %copy-start.3 = (bf16[128,2048]{1,0:T(8,128)(2,1)S(1)}, bf16[128,2048]{1,0:T(8,128)(2,1)}, u32[]{:S(2)}) copy-start(bf16[128,2048]{1,0:T(8,128)(2,1)} %copy-done.2) | copy-start | bytes 1572868
  303.6 235.1 %all-gather.8.cloned.1.call-start = ((), (), s32[]{:S(2)}) async-start(), calls=%async_computation.6 | async-start | bytes 8921088 | tf_op jit(solution)/shard_map/all_gather | solution.py:11
  304.3 93.1 %copy-start.7 = (bf16[128,2048]{1,0:T(8,128)(2,1)S(1)}, bf16[128,2048]{1,0:T(8,128)(2,1)}, u32[]{:S(2)}) copy-start(bf16[128,2048]{1,0:T(8,128)(2,1)} %param.21) | copy-start | bytes 1572868
  306.4 114.8 %copy-start.1 = (bf16[128,2048]{1,0:T(8,128)(2,1)S(1)}, bf16[128,2048]{1,0:T(8,128)(2,1)}, u32[]{:S(2)}) copy-start(bf16[128,2048]{1,0:T(8,128)(2,1)} %param.19) | copy-start | bytes 1572868
  306.4 48.2 %all-to-all-start = ((bf16[128,32,64]{0,2,1:T(8,128)(2,1)}), bf16[128,32,64]{0,2,1:T(8,128)(2,1)S(1)}, u32[]{:S(2)}, u32[]{:S(2)}) async-start(bf16[128,32,64]{0,2,1:T(8,128)(2,1)} %bitcast.3), calls=%async_computation | async-start | bytes 1048576 | tf_op jit(solution)/shard_map/all_to_all | solution.py:142
  354.6 82.4 %copy-start.9 = (bf16[128,2048]{1,0:T(8,128)(2,1)S(1)}, bf16[128,2048]{1,0:T(8,128)(2,1)}, u32[]{:S(2)}) copy-start(bf16[128,2048]{1,0:T(8,128)(2,1)} %copy-done.8) | copy-start | bytes 1572868
  354.6 37.7 %all-to-all-start.2 = ((bf16[128,32,64]{0,2,1:T(8,128)(2,1)}), bf16[128,32,64]{0,2,1:T(8,128)(2,1)S(1)}, u32[]{:S(2)}, u32[]{:S(2)}) async-start(bf16[128,32,64]{0,2,1:T(8,128)(2,1)} %bitcast.7), calls=%async_computation.2 | async-start | bytes 1048576 | tf_op jit(solution)/shard_map/all_to_all | solution.py:137
  392.3 38.6 %all-to-all-start.1 = ((bf16[128,32,64]{0,2,1:T(8,128)(2,1)}), bf16[128,32,64]{0,2,1:T(8,128)(2,1)}, u32[]{:S(2)}, u32[]{:S(2)}) async-start(bf16[128,32,64]{0,2,1:T(8,128)(2,1)} %bitcast.5), calls=%async_computation.1 | async-start | bytes 1048576 | tf_op jit(solution)/shard_map/all_to_all | solution.py:143
  398.4 140.3 %copy-start.13 = (f32[64,176]{1,0:T(8,128)S(1)}, f32[64,176]{1,0:T(8,128)}, u32[]{:S(2)}) copy-start(f32[64,176]{1,0:T(8,128)} %param.30) | copy-start | bytes 135172
  430.9 120.8 %all-to-all-start.3 = ((bf16[128,32,64]{0,2,1:T(8,128)(2,1)}), bf16[128,32,64]{0,2,1:T(8,128)(2,1)S(1)}, u32[]{:S(2)}, u32[]{:S(2)}) async-start(bf16[128,32,64]{0,2,1:T(8,128)(2,1)} %bitcast.9), calls=%async_computation.3 | async-start | bytes 1048576 | tf_op jit(solution)/shard_map/all_to_all | solution.py:138
  437.0 104.2 %copy-start.14 = (f32[64,176]{1,0:T(8,128)S(1)}, f32[64,176]{1,0:T(8,128)}, u32[]{:S(2)}) copy-start(f32[64,176]{1,0:T(8,128)} %param.31) | copy-start | bytes 135172
  439.8 104.0 %copy-start.15 = (f32[64,176]{1,0:T(8,128)S(1)}, f32[64,176]{1,0:T(8,128)}, u32[]{:S(2)}) copy-start(f32[64,176]{1,0:T(8,128)} %param.33) | copy-start | bytes 135172
  439.8 106.6 %copy-start.16 = (f32[64,176]{1,0:T(8,128)S(1)}, f32[64,176]{1,0:T(8,128)}, u32[]{:S(2)}) copy-start(f32[64,176]{1,0:T(8,128)} %param.34) | copy-start | bytes 135172
  541.2 7.8 %copy-start.17 = (f32[176,64]{0,1:T(8,128)S(1)}, f32[176,64]{0,1:T(8,128)}, u32[]{:S(2)}) copy-start(f32[176,64]{0,1:T(8,128)} %param.32) | copy-start | bytes 135172
  (4 other events, 13.0 us)
Sparse Core Ops, SparseCore 0:
  10.7 76.7 all-gather.5
  90.1 69.8 all-gather.3
  174.2 113.2 all-reduce.6
  303.7 117.5 all-reduce.4
  423.1 115.4 all-gather.7
where the time goes:
time: 562 us; the launch traced here: 561 us
  waiting for transfers between devices  447 us (80%)
  matrix products  41.5 us (7%)
  starting transfers between devices  30.4 us (5%)
  other arithmetic  22 us (4%)
  between operations  14 us (2%)
  local copies, waits for them, and re-layouts  6.1 us (1%)
    all_gather x2, waiting for transfers between devices, sent_together(): whole, at, outs = (lax.all_gather(both, axis, axis=dim, tiled=True), 0, [])  169 us
    psum x2, waiting for transfers between devices, block_forward(): lax.psum(jnp.dot(hidden, w_down, preferred_element_type=jnp.float32).asty...  133 us
    all_gather x1, waiting for transfers between devices, gather_turned(): whole = lax.all_gather(both, axis, axis=0, tiled=True)  71.3 us
    all_to_all x1, waiting for transfers between devices, per_device(): lax.all_to_all(saved_second[0], 'fs', split_axis=1, concat_axis=0, tiled=...  32.5 us
    all_to_all x1, waiting for transfers between devices, per_device(): lax.all_to_all(saved_first[0], 'fs', split_axis=1, concat_axis=0, tiled=T...  32.5 us
    all_to_all x1, starting transfers between devices, per_device(): lax.all_to_all(saved_first[0], 'fs', split_axis=1, concat_axis=0, tiled=T...  14.7 us
  transfers between devices with their start and end apart: 9, of which 8 were waited for; matrix products, arithmetic and copies ran while one was open for 6% of the time, Pallas kernels for 0%

commit v1 on v0

--- a/solution.py
+++ b/solution.py
@@ -19,7 +19,12 @@
     turned = [jnp.moveaxis(a, dim, 0) for a, dim in zip(arrays, dims)]
     widths = [t[0].size for t in turned]
     both = jnp.concatenate([t.reshape(-1, w) for t, w in zip(turned, widths)], axis=1)
-    whole = lax.all_gather(both, axis, axis=0, tiled=True)
+    whole = jnp.concatenate(
+        jax.lax.all_to_all(
+            jnp.stack([both] * jax.lax.axis_size(axis)), axis_name=axis, split_axis=0, concat_axis=0
+        ),
+        axis=0,
+    )
     blocks = jnp.split(whole, [sum(widths[:k]) for k in range(1, len(widths))], axis=1)
     return tuple(
         (

time: 562 us -> 531 us (0.945)
  waiting for transfers between devices: 447 us -> 403 us
  starting transfers between devices: 30.4 us -> 47 us
    all_to_all x0 -> x1, waiting for transfers between devices: none -> 82.9 us  [gather_turned(): jax.lax.all_to_all(jnp.stack([both] * jax.lax.axis_size(axis)), axis_name...]
    all_gather x1 -> x0, waiting for transfers between devices: 71.3 us -> none  [gather_turned(): whole = lax.all_gather(both, axis, axis=0, tiled=True)]
    all_gather x2, waiting for transfers between devices: 169 us -> 113 us  [sent_together(): whole, at, outs = (lax.all_gather(both, axis, axis=dim, tiled=True), 0, [])]
    all_to_all x0 -> x1, starting transfers between devices: none -> 16.7 us  [gather_turned(): jax.lax.all_to_all(jnp.stack([both] * jax.lax.axis_size(axis)), axis_name...]
where the time goes in v1:
time: 531 us; the launch traced here: 530 us
  waiting for transfers between devices  403 us (76%)
  starting transfers between devices  47 us (9%)
  matrix products  41.5 us (8%)
  other arithmetic  16.5 us (3%)
  between operations  14.1 us (3%)
  local copies, waits for them, and re-layouts  7.52 us (1%)
    psum x2, waiting for transfers between devices, block_forward(): lax.psum(jnp.dot(hidden, w_down, preferred_element_type=jnp.float32).asty...  134 us
    all_gather x2, waiting for transfers between devices, sent_together(): whole, at, outs = (lax.all_gather(both, axis, axis=dim, tiled=True), 0, [])  113 us
    all_to_all x1, waiting for transfers between devices, gather_turned(): jax.lax.all_to_all(jnp.stack([both] * jax.lax.axis_size(axis)), axis_name...  82.9 us
    all_to_all x1, waiting for transfers between devices, per_device(): lax.all_to_all(saved_second[0], 'fs', split_axis=1, concat_axis=0, tiled=...  32.5 us
    all_to_all x1, waiting for transfers between devices, per_device(): lax.all_to_all(saved_first[0], 'fs', split_axis=1, concat_axis=0, tiled=T...  32.5 us
    all_to_all x1, starting transfers between devices, gather_turned(): jax.lax.all_to_all(jnp.stack([both] * jax.lax.axis_size(axis)), axis_name...  16.7 us
    all_to_all x1, starting transfers between devices, per_device(): lax.all_to_all(saved_first[0], 'fs', split_axis=1, concat_axis=0, tiled=T...  14.7 us
  transfers between devices with their start and end apart: 9, of which 8 were waited for; matrix products, arithmetic and copies ran while one was open for 6% of the time, Pallas kernels for 0%

profile of v1, /device:TPU:1, one launch (start us, length us, event | category | flops | bytes accessed | tf_op | source)
XLA Modules:
  0.0 529.8 jit_solution(63431844227966916)
XLA Ops:
  9.6 16.7 %all-to-all-start = ((bf16[32,64,352]{2,1,0:T(8,128)(2,1)}), bf16[32,64,352]{2,1,0:T(8,128)(2,1)S(1)}, u32[]{:S(2)}, u32[]{:S(2)}) async-start(bf16[32,64,352]{2,1,0:T(8,128)(2,1)} %stack.2), calls=%async_computation | async-start | bytes 3145728 | tf_op jit(solution)/shard_map/all_to_all | solution.py:23
  28.9 82.9 %all-to-all-done = bf16[32,64,352]{2,1,0:T(8,128)(2,1)S(1)} async-done(((bf16[32,64,352]{2,1,0:T(8,128)(2,1)}), bf16[32,64,352]{2,1,0:T(8,128)(2,1)S(1)}, u32[]{:S(2)}, u32[]{:S(2)}) %all-to-all-start) | async-done | bytes 1441824 | tf_op jit(solution)/shard_map/all_to_all | solution.py:23
  114.0 14.1 %all-gather.3.cloned.1.call-done = bf16[2048,704]{1,0:T(8,128)(2,1)} async-done(((bf16[64,704]{1,0:T(8,128)(2,1)}), bf16[2048,704]{1,0:T(8,128)(2,1)}) %all-gather.3.cloned.1.call-update) | async-done | bytes 2883600 | tf_op jit(solution)/shard_map/all_gather | solution.py:11
  128.1 2.6 fusion.74
  130.7 3.2 constant_dynamic-update-slice_fusion.3
  136.2 3.9 convolution_convert_fusion.1
  145.6 110.9 %all-reduce.7.cloned.1.call-done = (bf16[128,2048]{1,0:T(8,128)(2,1)}, bf16[128,2048]{1,0:T(8,128)(2,1)}) async-done(((bf16[128,2048]{1,0:T(8,128)(2,1)}, bf16[128,2048]{1,0:T(8,128)(2,1)}), (bf16[128,2048]{1,0:T(8,128)(2,1)}, bf16[128,2048]{1,0:T(8,128)(2,1)})) %all-reduce.7.cloned.1.call-update) | async-done | bytes 1048592 | tf_op jit(solution)/shard_map/psum | solution.py:50
  266.5 4.0 convolution_convert_fusion
  275.3 14.7 %all-to-all-start.1 = ((bf16[128,32,64]{0,2,1:T(8,128)(2,1)}), bf16[128,32,64]{0,2,1:T(8,128)(2,1)S(1)}, u32[]{:S(2)}, u32[]{:S(2)}) async-start(bf16[128,32,64]{0,2,1:T(8,128)(2,1)} %bitcast.4), calls=%async_computation.1 | async-start | bytes 1048576 | tf_op jit(solution)/shard_map/all_to_all | solution.py:147
  291.0 32.5 %all-to-all-done.1 = bf16[128,32,64]{0,2,1:T(8,128)(2,1)S(1)} async-done(((bf16[128,32,64]{0,2,1:T(8,128)(2,1)}), bf16[128,32,64]{0,2,1:T(8,128)(2,1)S(1)}, u32[]{:S(2)}, u32[]{:S(2)}) %all-to-all-start.1) | async-done | bytes 524320 | tf_op jit(solution)/shard_map/all_to_all | solution.py:147
  323.5 4.2 all-to-all-start.3
  328.7 32.5 %all-to-all-done.3 = bf16[128,32,64]{0,2,1:T(8,128)(2,1)S(1)} async-done(((bf16[128,32,64]{0,2,1:T(8,128)(2,1)}), bf16[128,32,64]{0,2,1:T(8,128)(2,1)S(1)}, u32[]{:S(2)}, u32[]{:S(2)}) %all-to-all-start.3) | async-done | bytes 524320 | tf_op jit(solution)/shard_map/all_to_all | solution.py:142
  361.2 5.0 all-to-all-start.2
  367.3 22.9 %all-reduce.5.cloned.1.call-done = (bf16[128,2048]{1,0:T(8,128)(2,1)}, bf16[128,2048]{1,0:T(8,128)(2,1)}) async-done(((bf16[128,2048]{1,0:T(8,128)(2,1)}, bf16[128,2048]{1,0:T(8,128)(2,1)}), (bf16[128,2048]{1,0:T(8,128)(2,1)}, bf16[128,2048]{1,0:T(8,128)(2,1)})) %all-reduce.5.cloned.1.call-update) | async-done | bytes 1048592 | tf_op jit(solution)/shard_map/psum | solution.py:50
  391.5 8.3 %all-to-all-done.2 = bf16[128,32,64]{0,2,1:T(8,128)(2,1)} async-done(((bf16[128,32,64]{0,2,1:T(8,128)(2,1)}), bf16[128,32,64]{0,2,1:T(8,128)(2,1)}, u32[]{:S(2)}, u32[]{:S(2)}) %all-to-all-start.2) | async-done | bytes 524320 | tf_op jit(solution)/shard_map/all_to_all | solution.py:148
  399.8 6.1 %all-to-all-start.4 = ((bf16[128,32,64]{0,2,1:T(8,128)(2,1)}), bf16[128,32,64]{0,2,1:T(8,128)(2,1)S(1)}, u32[]{:S(2)}, u32[]{:S(2)}) async-start(bf16[128,32,64]{0,2,1:T(8,128)(2,1)} %bitcast.10), calls=%async_computation.4 | async-start | bytes 1048576 | tf_op jit(solution)/shard_map/all_to_all | solution.py:143
  406.0 2.7 fusion.59
  408.7 98.8 %all-gather.5.cloned.1.call-done = bf16[4096,1056]{0,1:T(8,128)(2,1)} async-done(((bf16[128,1056]{0,1:T(8,128)(2,1)}), bf16[4096,1056]{0,1:T(8,128)(2,1)}) %all-gather.5.cloned.1.call-update) | async-done | bytes 8650768 | tf_op jit(solution)/shard_map/all_gather | solution.py:11
  507.5 2.6 fusion.23
  510.1 2.6 fusion.26
  512.7 2.6 fusion.35
  515.3 2.6 fusion.38
  518.0 2.7 fusion.32
  520.7 2.6 fusion.44
  (99 shorter events, 33.8 us)
Async XLA Ops:
  7.2 19.2 %copy-start.17 = (bf16[64,176]{1,0:T(8,128)(2,1)S(1)}, bf16[64,176]{1,0:T(8,128)(2,1)}, u32[]{:S(2)}) copy-start(bf16[64,176]{1,0:T(8,128)(2,1)} %param.28) | copy-start | bytes 67588
  7.2 19.2 %copy-start.18 = (bf16[64,176]{1,0:T(8,128)(2,1)S(1)}, bf16[64,176]{1,0:T(8,128)(2,1)}, u32[]{:S(2)}) copy-start(bf16[64,176]{1,0:T(8,128)(2,1)} %param.27) | copy-start | bytes 67588
  7.2 20.1 %copy-start.11 = (bf16[128,2048]{1,0:T(8,128)(2,1)S(1)}, bf16[128,2048]{1,0:T(8,128)(2,1)}, u32[]{:S(2)}) copy-start(bf16[128,2048]{1,0:T(8,128)(2,1)} %param.18) | copy-start | bytes 1572868
  7.2 20.3 %copy-start.1 = (bf16[128,2048]{1,0:T(8,128)(2,1)S(1)}, bf16[128,2048]{1,0:T(8,128)(2,1)}, u32[]{:S(2)}) copy-start(bf16[128,2048]{1,0:T(8,128)(2,1)} %param.20) | copy-start | bytes 1572868
  7.2 20.4 %copy-start.2 = (bf16[128,2048]{1,0:T(8,128)(2,1)S(1)}, bf16[128,2048]{1,0:T(8,128)(2,1)}, u32[]{:S(2)}) copy-start(bf16[128,2048]{1,0:T(8,128)(2,1)} %param.19) | copy-start | bytes 1572868
  8.2 19.7 %copy-start.15 = (f32[2048]{0:T(1024)S(1)}, f32[2048]{0:T(1024)}, u32[]{:S(2)}) copy-start(f32[2048]{0:T(1024)} %param.23) | copy-start | bytes 24580
  9.6 102.2 %all-to-all-start = ((bf16[32,64,352]{2,1,0:T(8,128)(2,1)}), bf16[32,64,352]{2,1,0:T(8,128)(2,1)S(1)}, u32[]{:S(2)}, u32[]{:S(2)}) async-start(bf16[32,64,352]{2,1,0:T(8,128)(2,1)} %stack.2), calls=%async_computation | async-start | bytes 3145728 | tf_op jit(solution)/shard_map/all_to_all | solution.py:23
  26.4 101.8 %all-gather.3.cloned.1.call-start = ((), (), s32[]{:S(2)}) async-start(), calls=%async_computation.5 | async-start | bytes 3244032 | tf_op jit(solution)/shard_map/all_gather | solution.py:11
  27.2 229.2 %all-reduce.7.cloned.1.call-start = ((), (), s32[]{:S(2)}) async-start(), calls=%async_computation.8 | async-start | bytes 2097152 | tf_op jit(solution)/shard_map/psum | solution.py:50
  28.9 105.7 %copy-start.16 = (f32[2048]{0:T(1024)S(1)}, f32[2048]{0:T(1024)}, u32[]{:S(2)}) copy-start(f32[2048]{0:T(1024)} %param.22) | copy-start | bytes 24580
  142.2 247.9 %all-reduce.5.cloned.1.call-start = ((), (), s32[]{:S(2)}) async-start(), calls=%async_computation.7 | async-start | bytes 2097152 | tf_op jit(solution)/shard_map/psum | solution.py:50
  272.4 55.3 %copy-start.5 = (bf16[128,2048]{1,0:T(8,128)(2,1)S(1)}, bf16[128,2048]{1,0:T(8,128)(2,1)}, u32[]{:S(2)}) copy-start(bf16[128,2048]{1,0:T(8,128)(2,1)} %copy-done.4) | copy-start | bytes 1572868
  272.5 235.1 %all-gather.5.cloned.1.call-start = ((), (), s32[]{:S(2)}) async-start(), calls=%async_computation.6 | async-start | bytes 8921088 | tf_op jit(solution)/shard_map/all_gather | solution.py:11
  273.2 93.0 %copy-start.12 = (bf16[128,2048]{1,0:T(8,128)(2,1)S(1)}, bf16[128,2048]{1,0:T(8,128)(2,1)}, u32[]{:S(2)}) copy-start(bf16[128,2048]{1,0:T(8,128)(2,1)} %param.21) | copy-start | bytes 1572868
  275.3 114.8 %copy-start.3 = (bf16[128,2048]{1,0:T(8,128)(2,1)S(1)}, bf16[128,2048]{1,0:T(8,128)(2,1)}, u32[]{:S(2)}) copy-start(bf16[128,2048]{1,0:T(8,128)(2,1)} %param.19) | copy-start | bytes 1572868
  275.3 48.2 %all-to-all-start.1 = ((bf16[128,32,64]{0,2,1:T(8,128)(2,1)}), bf16[128,32,64]{0,2,1:T(8,128)(2,1)S(1)}, u32[]{:S(2)}, u32[]{:S(2)}) async-start(bf16[128,32,64]{0,2,1:T(8,128)(2,1)} %bitcast.4), calls=%async_computation.1 | async-start | bytes 1048576 | tf_op jit(solution)/shard_map/all_to_all | solution.py:147
  323.5 82.4 %copy-start.14 = (bf16[128,2048]{1,0:T(8,128)(2,1)S(1)}, bf16[128,2048]{1,0:T(8,128)(2,1)}, u32[]{:S(2)}) copy-start(bf16[128,2048]{1,0:T(8,128)(2,1)} %copy-done.13) | copy-start | bytes 1572868
  323.5 37.7 %all-to-all-start.3 = ((bf16[128,32,64]{0,2,1:T(8,128)(2,1)}), bf16[128,32,64]{0,2,1:T(8,128)(2,1)S(1)}, u32[]{:S(2)}, u32[]{:S(2)}) async-start(bf16[128,32,64]{0,2,1:T(8,128)(2,1)} %bitcast.8), calls=%async_computation.3 | async-start | bytes 1048576 | tf_op jit(solution)/shard_map/all_to_all | solution.py:142
  361.2 38.6 %all-to-all-start.2 = ((bf16[128,32,64]{0,2,1:T(8,128)(2,1)}), bf16[128,32,64]{0,2,1:T(8,128)(2,1)}, u32[]{:S(2)}, u32[]{:S(2)}) async-start(bf16[128,32,64]{0,2,1:T(8,128)(2,1)} %bitcast.6), calls=%async_computation.2 | async-start | bytes 1048576 | tf_op jit(solution)/shard_map/all_to_all | solution.py:148
  367.3 140.3 %copy-start.21 = (f32[64,176]{1,0:T(8,128)S(1)}, f32[64,176]{1,0:T(8,128)}, u32[]{:S(2)}) copy-start(f32[64,176]{1,0:T(8,128)} %param.30) | copy-start | bytes 135172
  399.8 120.8 %all-to-all-start.4 = ((bf16[128,32,64]{0,2,1:T(8,128)(2,1)}), bf16[128,32,64]{0,2,1:T(8,128)(2,1)S(1)}, u32[]{:S(2)}, u32[]{:S(2)}) async-start(bf16[128,32,64]{0,2,1:T(8,128)(2,1)} %bitcast.10), calls=%async_computation.4 | async-start | bytes 1048576 | tf_op jit(solution)/shard_map/all_to_all | solution.py:143
  405.9 104.2 %copy-start.22 = (f32[64,176]{1,0:T(8,128)S(1)}, f32[64,176]{1,0:T(8,128)}, u32[]{:S(2)}) copy-start(f32[64,176]{1,0:T(8,128)} %param.31) | copy-start | bytes 135172
  408.7 104.0 %copy-start.23 = (f32[64,176]{1,0:T(8,128)S(1)}, f32[64,176]{1,0:T(8,128)}, u32[]{:S(2)}) copy-start(f32[64,176]{1,0:T(8,128)} %param.33) | copy-start | bytes 135172
  408.7 106.6 %copy-start.24 = (f32[64,176]{1,0:T(8,128)S(1)}, f32[64,176]{1,0:T(8,128)}, u32[]{:S(2)}) copy-start(f32[64,176]{1,0:T(8,128)} %param.34) | copy-start | bytes 135172
  (12 other events, 98.7 us)
Sparse Core Ops, SparseCore 0:
  29.9 98.2 all-gather.2
  142.3 114.0 all-reduce.6
  272.6 117.5 all-reduce.4
  392.0 115.4 all-gather.4
